TPU v7x, 32 devices: a whole 2x2x4 slice. The times are simulated.
32 devices in a mesh: rep: 2 (over y), fs: 4 (over z), tp: 4 (over x, core).
Axes of the slice: x: 2, y: 2, z: 4, core: 2. Of those that a mesh axis runs over, the one named last changes fastest.
Arguments:
- activations: bfloat16 [3072, 2048], P(('rep', 'fs'), 'tp'), may hold values from -16 to 16
- norm_gain: float32 [2048], replicated, may hold values from 0.1 to 1.9
- query_weight: bfloat16 [2048, 512], P('fs', 'tp'), may hold values from -0.125 to 0.125
- key_weight: bfloat16 [2048, 512], P('fs', 'tp'), may hold values from -0.125 to 0.125
- value_weight: bfloat16 [2048, 512], P('fs', 'tp'), may hold values from -0.125 to 0.125
- gate_weight: bfloat16 [2048, 512], P('fs', 'tp'), may hold values from -0.125 to 0.125
- out_weight: bfloat16 [512, 2048], P('tp', 'fs'), may hold values from -0.25 to 0.25
- mlp_gain: float32 [2048], replicated, may hold values from 0.1 to 1.9
- up_weight: bfloat16 [2048, 8192], P('fs', 'tp'), may hold values from -0.125 to 0.125
- down_weight: bfloat16 [8192, 2048], P('tp', 'fs'), may hold values from -0.0625 to 0.0625
Outputs:
- layer_out: bfloat16 [3072, 2048], P(('rep', 'fs'), 'tp')
All inputs are finite; a program needn't handle non-finite values.
Results may differ from a plain program's by a relative error of at most 0.012.
Values may be sent and summed in bfloat16 or wider, within the bound.
A program may use at most 64 MiB of HBM per device.

v0:
```python
import jax
import jax.numpy as jnp
from jax import lax
from jax.sharding import PartitionSpec as P

HEADS = 8
HEAD_DIM = 64
BLOCK = 64
SEQ_LEN = 128
EPSILON = 1e-06


def rms_norm(rows, gain):
    floats = rows.astype(jnp.float32)
    scaled = floats * lax.rsqrt(jnp.mean(floats * floats, axis=-1, keepdims=True) + EPSILON)
    return (scaled * gain).astype(jnp.bfloat16)


def rotate(raw, cosine, sine, seqs, heads):
    half = HEAD_DIM // 2
    shaped = raw.reshape(seqs, SEQ_LEN, heads, HEAD_DIM)
    first, second = (shaped[..., :half], shaped[..., half:])
    return jnp.concatenate(
        [first * cosine - second * sine, second * cosine + first * sine], axis=-1
    )


def retain(query_raw, key_raw, value_rows, gate_rows, first_head):
    tokens = query_raw.shape[0]
    heads = query_raw.shape[1] // HEAD_DIM
    seqs = tokens // SEQ_LEN
    blocks = SEQ_LEN // BLOCK
    half = HEAD_DIM // 2
    position = jnp.arange(SEQ_LEN, dtype=jnp.float32)
    freqs = 10000.0 ** (-jnp.arange(half, dtype=jnp.float32) / half)
    angle = position[:, None] * freqs[None, :]
    cosine = jnp.cos(angle)[:, None, :]
    sine = jnp.sin(angle)[:, None, :]
    shape_five = (seqs, blocks, BLOCK, heads, HEAD_DIM)
    queries = rotate(query_raw, cosine, sine, seqs, heads).astype(jnp.bfloat16).reshape(shape_five)
    key_block = (
        (rotate(key_raw, cosine, sine, seqs, heads) * HEAD_DIM ** (-0.5))
        .astype(jnp.bfloat16)
        .reshape(shape_five)
    )
    value_block = value_rows.reshape(shape_five)
    head_index = first_head + jnp.arange(heads, dtype=jnp.float32)
    exponent = 5.0 + 4.0 * head_index / (HEADS - 1)
    log_gamma = jnp.log(1.0 - jnp.power(2.0, -exponent))
    offsets = jnp.arange(BLOCK, dtype=jnp.float32)
    distance = offsets[:, None] - offsets[None, :]
    decay_mask = jnp.where(
        distance[None] >= 0,
        jnp.exp(jnp.maximum(distance, 0.0)[None] * log_gamma[:, None, None]),
        0.0,
    )
    scores = jnp.einsum(
        "snbhd,snchd->snhbc", queries, key_block, preferred_element_type=jnp.float32
    )
    weights = (scores * decay_mask[None, None]).astype(jnp.bfloat16)
    inner = jnp.einsum(
        "snhbc,snchd->snbhd", weights, value_block, preferred_element_type=jnp.float32
    )
    query_decay = (
        queries.astype(jnp.float32)
        * jnp.exp((offsets + 1.0)[:, None] * log_gamma[None, :])[:, :, None]
    )
    key_decay = (
        key_block.astype(jnp.float32)
        * jnp.exp((BLOCK - 1.0 - offsets)[:, None] * log_gamma[None, :])[:, :, None]
    )
    block_decay = jnp.exp(BLOCK * log_gamma)[None, :, None, None]

    def advance(state, inputs):
        query_now, key_now, value_now = inputs
        carried = jnp.einsum("sbhd,shde->sbhe", query_now, state, precision=lax.Precision.HIGHEST)
        state = state * block_decay + jnp.einsum(
            "sbhd,sbhe->shde", key_now, value_now, precision=lax.Precision.HIGHEST
        )
        return (state, carried)

    initial = jnp.zeros((seqs, heads, HEAD_DIM, HEAD_DIM), jnp.float32)
    _, cross = lax.scan(
        advance,
        initial,
        (
            jnp.moveaxis(query_decay, 1, 0),
            jnp.moveaxis(key_decay, 1, 0),
            jnp.moveaxis(value_block.astype(jnp.float32), 1, 0),
        ),
    )
    mixed = (inner + jnp.moveaxis(cross, 0, 1)).reshape(tokens, heads, HEAD_DIM)
    centred = mixed - jnp.mean(mixed, axis=-1, keepdims=True)
    normed = centred * lax.rsqrt(jnp.mean(centred * centred, axis=-1, keepdims=True) + EPSILON)
    gated = normed * jax.nn.silu(gate_rows.reshape(tokens, heads, HEAD_DIM))
    return gated.reshape(tokens, heads * HEAD_DIM).astype(jnp.bfloat16)


def local(
    activations,
    norm_gain,
    query_weight,
    key_weight,
    value_weight,
    gate_weight,
    out_weight,
    mlp_gain,
    up_weight,
    down_weight,
):
    full_rows = lax.all_gather(activations, "tp", axis=1, tiled=True)
    normed = rms_norm(full_rows, norm_gain)
    head_width = query_weight.shape[1]
    pieces = (
        lax.all_gather(query_weight, "fs", axis=0, tiled=True),
        lax.all_gather(key_weight, "fs", axis=0, tiled=True),
        lax.all_gather(value_weight, "fs", axis=0, tiled=True),
        lax.all_gather(gate_weight, "fs", axis=0, tiled=True),
    )
    columns = normed
    query_raw, key_raw, value_raw, gate_rows = tuple(
        (jnp.dot(columns, piece, preferred_element_type=jnp.float32) for piece in pieces)
    )
    first_head = (lax.axis_index("tp") * (head_width // HEAD_DIM)).astype(jnp.float32)
    retained = retain(query_raw, key_raw, value_raw.astype(jnp.bfloat16), gate_rows, first_head)
    out_rows = lax.all_gather(out_weight, "fs", axis=1, tiled=True)
    out_mine = lax.all_to_all(out_rows, "tp", split_axis=1, concat_axis=0, tiled=True)
    branch = jnp.dot(
        lax.all_gather(retained, "tp", axis=1, tiled=True),
        out_mine,
        preferred_element_type=jnp.float32,
    )
    middle = (activations.astype(jnp.float32) + branch).astype(jnp.bfloat16)
    middle_rows = lax.all_gather(middle, "tp", axis=1, tiled=True)
    second = rms_norm(middle_rows, mlp_gain)
    columns = second
    up_rows = jnp.dot(
        columns,
        lax.all_gather(up_weight, "fs", axis=0, tiled=True),
        preferred_element_type=jnp.float32,
    )
    hidden = jnp.square(jax.nn.relu(up_rows)).astype(jnp.bfloat16)
    down_part = jnp.dot(
        hidden,
        lax.all_gather(down_weight, "fs", axis=1, tiled=True),
        preferred_element_type=jnp.float32,
    )
    summed = lax.psum_scatter(
        down_part.astype(jnp.bfloat16), "tp", scatter_dimension=1, tiled=True
    ).astype(jnp.float32)
    return (middle.astype(jnp.float32) + summed).astype(jnp.bfloat16)


def solution(mesh):
    in_specs = (
        P(("rep", "fs"), "tp"),
        P(),
        P("fs", "tp"),
        P("fs", "tp"),
        P("fs", "tp"),
        P("fs", "tp"),
        P("tp", "fs"),
        P(),
        P("fs", "tp"),
        P("tp", "fs"),
    )
    out_specs = P(("rep", "fs"), "tp")
    return jax.shard_map(local, mesh=mesh, in_specs=in_specs, out_specs=out_specs, check_vma=False)
```

profile of v0, /device:TPU:0, one launch (start us, length us, event | category | flops | bytes accessed | tf_op | source)
XLA Modules:
  0.0 495.4 jit_solution(16043336632377507980)
XLA Ops:
  6.5 0.7 all-gather.5.cloned.1.call-update
  7.3 1.1 copy.70
  8.3 18.0 %all_gather.36 = bf16[128,2048]{0,1:T(8,128)(2,1)} all-gather(bf16[128,512]{0,1:T(8,128)(2,1)S(1)} %copy.70), channel_id=1, replica_groups=mesh['rep'=2,'fs'=4,'tp'=4] {'fs'}, dimensions={1}, use_global_device_ids=true | all-gather | bytes 655360 | tf_op jit(solution)/shard_map/all_gather | solution.py:126
  26.3 3.5 all-to-all-start
  30.0 17.0 %all_gather.32 = bf16[2048,128]{1,0:T(8,128)(2,1)S(1)} all-gather(bf16[512,128]{1,0:T(8,128)(2,1)S(1)} %copy-done.7), channel_id=1, replica_groups=mesh['rep'=2,'fs'=4,'tp'=4] {'fs'}, dimensions={0}, use_global_device_ids=true | all-gather | bytes 655360 | tf_op jit(solution)/shard_map/all_gather | solution.py:115
  47.0 16.0 %all_gather.33 = bf16[2048,128]{1,0:T(8,128)(2,1)S(1)} all-gather(bf16[512,128]{1,0:T(8,128)(2,1)S(1)} %copy-done.8), channel_id=1, replica_groups=mesh['rep'=2,'fs'=4,'tp'=4] {'fs'}, dimensions={0}, use_global_device_ids=true | all-gather | bytes 655360 | tf_op jit(solution)/shard_map/all_gather | solution.py:116
  63.0 16.3 %all_gather.31 = bf16[2048,128]{1,0:T(8,128)(2,1)S(1)} all-gather(bf16[512,128]{1,0:T(8,128)(2,1)S(1)} %copy-done.9), channel_id=1, replica_groups=mesh['rep'=2,'fs'=4,'tp'=4] {'fs'}, dimensions={0}, use_global_device_ids=true | all-gather | bytes 655360 | tf_op jit(solution)/shard_map/all_gather | solution.py:117
  79.2 0.7 multiply_exponential_fusion
  79.9 0.7 fusion.34
  80.7 15.5 %all_gather.34 = bf16[2048,128]{1,0:T(8,128)(2,1)} all-gather(bf16[512,128]{1,0:T(8,128)(2,1)S(1)} %copy-done.10), channel_id=1, replica_groups=mesh['rep'=2,'fs'=4,'tp'=4] {'fs'}, dimensions={0}, use_global_device_ids=true | all-gather | bytes 655360 | tf_op jit(solution)/shard_map/all_gather | solution.py:118
  96.1 0.7 exponential_select_fusion
  96.9 1.0 copy.71
  97.9 1.9 fusion.14
  99.8 0.4 fusion.16
  100.2 0.6 fusion.40
  100.9 0.6 fusion.41
  101.6 0.8 subtract_convert_fusion
  102.9 0.2 reshape.277
  103.1 0.2 copy.58
  103.3 1.1 reshape.278
  104.4 0.9 copy.59
  105.3 0.6 convolution_convert_fusion.1
  106.1 0.6 copy-done.4
  106.9 1.9 multiply_bitcast_fusion.1
  108.7 3.4 while.13
  108.7 0.3 convolution_bitcast_fusion.3
  109.2 0.7 constant_dynamic-update-slice_fusion.2
  109.9 0.5 convolution_add_fusion.3
  110.4 0.3 convolution_bitcast_fusion.3
  110.9 0.7 constant_dynamic-update-slice_fusion.2
  111.6 0.5 convolution_add_fusion.3
  112.1 1.8 fusion.39
  114.0 0.2 copy.65
  114.3 0.9 reshape.274
  115.6 0.8 copy.67
  116.4 1.6 multiply_convert_fusion.1
  118.0 6.8 %all_gather.35 = bf16[384,512]{1,0:T(8,128)(2,1)S(1)} all-gather(bf16[384,128]{1,0:T(8,128)(2,1)S(1)} %multiply_convert_fusion.1), channel_id=1, replica_groups=mesh['rep'=2,'fs'=4,'tp'=4] {'tp'}, dimensions={1}, use_global_device_ids=true | all-gather | bytes 491520 | tf_op jit(solution)/shard_map/all_gather | solution.py:129
  124.9 1.1 fusion.23
  126.1 0.7 all-gather.11.cloned.1.call-update
  126.8 0.5 all-gather.9.cloned.1.call-update
  127.3 0.2 reduce-scatter.2.cloned.1.call-start
  127.6 18.5 %all-gather.7.cloned.1.call-done = bf16[384,2048]{1,0:T(8,128)(2,1)} async-done(((bf16[384,512]{1,0:T(8,128)(2,1)}), bf16[384,2048]{1,0:T(8,128)(2,1)}) %all-gather.7.cloned.1.call-update) | async-done | bytes 1572880 | tf_op jit(solution)/shard_map/all_gather | solution.py:134
  146.0 1.8 fusion.17
  147.9 149.4 %all-gather.11.cloned.1.call-done = bf16[2048,2048]{1,0:T(8,128)(2,1)} async-done(((bf16[2048,512]{1,0:T(8,128)(2,1)}), bf16[2048,2048]{1,0:T(8,128)(2,1)}) %all-gather.11.cloned.1.call-update) | async-done | bytes 8388624 | tf_op jit(solution)/shard_map/all_gather | solution.py:145
  297.3 149.3 %all-gather.9.cloned.1.call-done = bf16[2048,2048]{1,0:T(8,128)(2,1)} async-done(((bf16[512,2048]{1,0:T(8,128)(2,1)}), bf16[2048,2048]{1,0:T(8,128)(2,1)}) %all-gather.9.cloned.1.call-update) | async-done | bytes 8388624 | tf_op jit(solution)/shard_map/all_gather | solution.py:139
  446.5 14.1 %convolution_convert_fusion = bf16[384,2048]{1,0:T(8,128)(2,1)} fusion(bf16[2048,2048]{1,0:T(8,128)(2,1)} %all-gather.11.cloned.1.call-done, bf16[2048,2048]{1,0:T(8,128)(2,1)} %all-gather.9.cloned.1.call-done, bf16[384,2048]{1,0:T(8,128)(2,1)} %all-gather.7.cloned.1.call-done, f32[2048]{0:T(1024)S(1)} %copy-done.15, f32[384]{0:T(512)S(1)} %add_rsqrt_fusion.1), kind=kOutput, calls=%fused_computation.28 | convolution fusion | flops 6448742400 | bytes 19932672 | tf_op jit(solution)/shard_map/dot_general | solution.py:143
  460.6 26.4 %reduce-scatter.2.cloned.1.call-done = bf16[384,512]{1,0:T(8,128)(2,1)} async-done(((bf16[384,2048]{1,0:T(8,128)(2,1)}), bf16[384,512]{1,0:T(8,128)(2,1)}) %reduce-scatter.2.cloned.1.call-update) | async-done | bytes 393232 | tf_op jit(solution)/shard_map/reduce_scatter | solution.py:148
  487.0 1.8 add_convert_fusion
  (71 shorter events, 2.0 us)
Async XLA Ops:
  6.5 23.5 %copy-start.7 = (bf16[512,128]{1,0:T(8,128)(2,1)S(1)}, bf16[512,128]{1,0:T(8,128)(2,1)}, u32[]{:S(2)}) copy-start(bf16[512,128]{1,0:T(8,128)(2,1)} %param.14) | copy-start | bytes 393220
  6.5 40.5 %copy-start.8 = (bf16[512,128]{1,0:T(8,128)(2,1)S(1)}, bf16[512,128]{1,0:T(8,128)(2,1)}, u32[]{:S(2)}) copy-start(bf16[512,128]{1,0:T(8,128)(2,1)} %param.15) | copy-start | bytes 393220
  6.5 56.4 %copy-start.9 = (bf16[512,128]{1,0:T(8,128)(2,1)S(1)}, bf16[512,128]{1,0:T(8,128)(2,1)}, u32[]{:S(2)}) copy-start(bf16[512,128]{1,0:T(8,128)(2,1)} %param.16) | copy-start | bytes 393220
  6.5 91.3 %all-gather.5.cloned.1.call-start = ((), (), s32[]{:S(2)}) async-start(), calls=%async_computation.2 | async-start | bytes 1966080 | tf_op jit(solution)/shard_map/all_gather | solution.py:111
  7.3 73.4 %copy-start.10 = (bf16[512,128]{1,0:T(8,128)(2,1)S(1)}, bf16[512,128]{1,0:T(8,128)(2,1)}, u32[]{:S(2)}) copy-start(bf16[512,128]{1,0:T(8,128)(2,1)} %param.17) | copy-start | bytes 393220
  26.3 70.5 %all-to-all-start = ((bf16[128,4,512]{0,2,1:T(8,128)(2,1)}), bf16[128,4,512]{0,2,1:T(8,128)(2,1)S(1)}, u32[]{:S(2)}, u32[]{:S(2)}) async-start(bf16[128,4,512]{0,2,1:T(8,128)(2,1)} %bitcast.7), calls=%async_computation | async-start | bytes 1048576 | tf_op jit(solution)/shard_map/all_to_all | solution.py:127
  29.8 116.2 %all-gather.7.cloned.1.call-start = ((), (), s32[]{:S(2)}) async-start(), calls=%async_computation.3 | async-start | bytes 1966080 | tf_op jit(solution)/shard_map/all_gather | solution.py:134
  62.9 36.8 %copy-start.12 = (f32[2048]{0:T(1024)S(1)}, f32[2048]{0:T(1024)}, u32[]{:S(2)}) copy-start(f32[2048]{0:T(1024)} %param.13) | copy-start | bytes 24580
  97.9 1.9 copy-start
  100.8 0.8 copy-start.11
  102.9 3.8 copy-start.3
  103.3 3.4 copy-start.14
  104.4 2.5 copy-start.13
  106.0 0.7 copy-start.4
  112.1 4.3 copy-start.6
  115.5 9.4 %copy-start.2 = (bf16[4,128,512]{2,1,0:T(8,128)(2,1)S(1)}, bf16[4,128,512]{2,1,0:T(8,128)(2,1)}, u32[]{:S(2)}) copy-start(bf16[4,128,512]{2,1,0:T(8,128)(2,1)} %copy.71) | copy-start | bytes 1572868
  115.5 9.4 %copy-start.5 = (bf16[384,512]{1,0:T(8,128)(2,1)S(1)}, bf16[384,512]{1,0:T(8,128)(2,1)}, u32[]{:S(2)}) copy-start(bf16[384,512]{1,0:T(8,128)(2,1)} %param.12) | copy-start | bytes 1179652
  126.0 171.2 %all-gather.11.cloned.1.call-start = ((), (), s32[]{:S(2)}) async-start(), calls=%async_computation.5 | async-start | bytes 10485760 | tf_op jit(solution)/shard_map/all_gather | solution.py:145
  126.8 319.8 %copy-start.15 = (f32[2048]{0:T(1024)S(1)}, f32[2048]{0:T(1024)}, u32[]{:S(2)}) copy-start(f32[2048]{0:T(1024)} %param.19) | copy-start | bytes 24580
  126.8 319.8 %all-gather.9.cloned.1.call-start = ((), (), s32[]{:S(2)}) async-start(), calls=%async_computation.4 | async-start | bytes 10485760 | tf_op jit(solution)/shard_map/all_gather | solution.py:139
  127.3 359.7 %reduce-scatter.2.cloned.1.call-start = ((), (), s32[]{:S(2)}) async-start(), calls=%async_computation.6 | async-start | bytes 1966080 | tf_op jit(solution)/shard_map/reduce_scatter | solution.py:148
  147.8 339.2 %copy-start.1 = (bf16[384,512]{1,0:T(8,128)(2,1)S(1)}, bf16[384,512]{1,0:T(8,128)(2,1)}, u32[]{:S(2)}) copy-start(bf16[384,512]{1,0:T(8,128)(2,1)} %fusion.23) | copy-start | bytes 1179652
Sparse Core Ops, SparseCore 0:
  8.9 22.3 all-gather.4
  126.1 19.8 all-gather.6
  147.6 149.5 all-gather.10
  298.7 147.7 all-gather.8
  460.8 26.1 reduce-scatter.1
where the time goes:
time: 496 us; the launch traced here: 495 us
  waiting for transfers between devices  345 us (70%)
  blocking collectives  89.6 us (18%)
  matrix products  22 us (4%)
  between operations  13.5 us (3%)
  other arithmetic  11.1 us (2%)
  local copies, waits for them, and re-layouts  9.82 us (2%)
    all_gather x1, waiting for transfers between devices, local(): lax.all_gather(down_weight, 'fs', axis=1, tiled=True)  149 us
    all_gather x1, waiting for transfers between devices, local(): lax.all_gather(up_weight, 'fs', axis=0, tiled=True)  149 us
    reduce_scatter x1, waiting for transfers between devices, local(): lax.psum_scatter(down_part.astype(jnp.bfloat16), 'tp', scatter_dimension=...  26.4 us
    all_gather x1, waiting for transfers between devices, local(): middle_rows = lax.all_gather(middle, 'tp', axis=1, tiled=True)  18.5 us
    all_gather x1, blocking collectives, local(): out_rows = lax.all_gather(out_weight, 'fs', axis=1, tiled=True)  18 us
    all_gather x1, blocking collectives, local(): lax.all_gather(query_weight, 'fs', axis=0, tiled=True)  17 us
    all_gather x1, blocking collectives, local(): lax.all_gather(value_weight, 'fs', axis=0, tiled=True)  16.3 us
    all_gather x1, blocking collectives, local(): lax.all_gather(key_weight, 'fs', axis=0, tiled=True)  16 us
  transfers between devices with their start and end apart: 6, of which 4 were waited for; matrix products, arithmetic and copies ran while one was open for 1% of the time, Pallas kernels for 0%

commit v1 on v0

--- a/solution.py
+++ b/solution.py
@@ -8,6 +8,22 @@
 BLOCK = 64
 SEQ_LEN = 128
 EPSILON = 1e-06
+
+
+def collect(x, axis, dim):
+    ways, here, step = (lax.axis_size(axis), lax.axis_index(axis), x.shape[dim])
+    shape = [n * ways if d == dim else n for d, n in enumerate(x.shape)]
+    full = lax.dynamic_update_slice_in_dim(jnp.zeros(shape, x.dtype), x, here * step, axis=dim)
+    going_up = going_down = x
+    for far in range(1, ways // 2 + 1):
+        going_up = lax.ppermute(going_up, axis, [(d, (d + 1) % ways) for d in range(ways)])
+        full = lax.dynamic_update_slice_in_dim(full, going_up, (here - far) % ways * step, axis=dim)
+        if 2 * far < ways:
+            going_down = lax.ppermute(going_down, axis, [(d, (d - 1) % ways) for d in range(ways)])
+            full = lax.dynamic_update_slice_in_dim(
+                full, going_down, (here + far) % ways * step, axis=dim
+            )
+    return full
 
 
 def rms_norm(rows, gain):
@@ -134,11 +150,7 @@
     middle_rows = lax.all_gather(middle, "tp", axis=1, tiled=True)
     second = rms_norm(middle_rows, mlp_gain)
     columns = second
-    up_rows = jnp.dot(
-        columns,
-        lax.all_gather(up_weight, "fs", axis=0, tiled=True),
-        preferred_element_type=jnp.float32,
-    )
+    up_rows = jnp.dot(columns, collect(up_weight, "fs", 0), preferred_element_type=jnp.float32)
     hidden = jnp.square(jax.nn.relu(up_rows)).astype(jnp.bfloat16)
     down_part = jnp.dot(
         hidden,

time: 496 us -> 453 us (0.913)
  waiting for transfers between devices: 345 us -> 256 us
  starting transfers between devices: 3.81 us -> 33 us
  local copies, waits for them, and re-layouts: 9.82 us -> 23.7 us
    ppermute x0 -> x3, waiting for transfers between devices: none -> 204 us  [the longest x1 109 us: collect(): lax.ppermute(going_down, axis, [(d, (d - 1) % ways) for d in range(ways)])]
    all_gather x1 -> x0, waiting for transfers between devices: 149 us -> none  [local(): lax.all_gather(up_weight, 'fs', axis=0, tiled=True)]
    all_gather x1, waiting for transfers between devices: 149 us -> 24.5 us  [local(): lax.all_gather(down_weight, 'fs', axis=1, tiled=True)]
    ppermute x0 -> x3, starting transfers between devices: none -> 29.3 us  [the longest x2 26.5 us: collect(): lax.ppermute(going_up, axis, [(d, (d + 1) % ways) for d in range(ways)])]
    all_gather x1, waiting for transfers between devices: 18.5 us -> 0.01 us  [local(): middle_rows = lax.all_gather(middle, 'tp', axis=1, tiled=True)]
    dynamic_update_slice x0 -> x4, local copies, waits for them, and re-layouts: none -> 11 us  [the longest x2 6.31 us: collect(): lax.dynamic_update_slice_in_dim(full, going_up, (here - far) % ways * ste...]
  transfers between devices with their start and end apart: 6 -> 8, of which waited for: 4 -> 5; matrix products, arithmetic and copies ran while one was open for 1% -> 5% of each run, Pallas kernels for 0% -> 0%
where the time goes in v1:
time: 453 us; the launch traced here: 452 us
  waiting for transfers between devices  256 us (57%)
  blocking collectives  89.8 us (20%)
  starting transfers between devices  33 us (7%)
  local copies, waits for them, and re-layouts  23.7 us (5%)
  matrix products  23 us (5%)
  between operations  13.5 us (3%)
  other arithmetic  12.4 us (3%)
    ppermute x1, waiting for transfers between devices, collect(): lax.ppermute(going_down, axis, [(d, (d - 1) % ways) for d in range(ways)])  109 us
    ppermute x2, waiting for transfers between devices, collect(): lax.ppermute(going_up, axis, [(d, (d + 1) % ways) for d in range(ways)])  94.8 us
    reduce_scatter x1, waiting for transfers between devices, local(): lax.psum_scatter(down_part.astype(jnp.bfloat16), 'tp', scatter_dimension=...  26.8 us
    ppermute x2, starting transfers between devices, collect(): lax.ppermute(going_up, axis, [(d, (d + 1) % ways) for d in range(ways)])  26.5 us
    all_gather x1, waiting for transfers between devices, local(): lax.all_gather(down_weight, 'fs', axis=1, tiled=True)  24.5 us
    all_gather x1, blocking collectives, local(): out_rows = lax.all_gather(out_weight, 'fs', axis=1, tiled=True)  18 us
    all_gather x1, blocking collectives, local(): lax.all_gather(query_weight, 'fs', axis=0, tiled=True)  17.2 us
    all_gather x1, blocking collectives, local(): lax.all_gather(key_weight, 'fs', axis=0, tiled=True)  15.8 us
  transfers between devices with their start and end apart: 8, of which 5 were waited for; matrix products, arithmetic and copies ran while one was open for 5% of the time, Pallas kernels for 0%

profile of v1, /device:TPU:0, one launch (start us, length us, event | category | flops | bytes accessed | tf_op | source)
XLA Modules:
  0.0 452.0 jit_solution(17411833199812975011)
XLA Ops:
  6.5 0.7 all-gather.4.cloned.1.call-update
  7.3 1.0 copy.70
  8.3 18.0 %all_gather.33 = bf16[128,2048]{0,1:T(8,128)(2,1)} all-gather(bf16[128,512]{0,1:T(8,128)(2,1)S(1)} %copy.70), channel_id=1, replica_groups=mesh['rep'=2,'fs'=4,'tp'=4] {'fs'}, dimensions={1}, use_global_device_ids=true | all-gather | bytes 655360 | tf_op jit(solution)/shard_map/all_gather | solution.py:142
  26.3 3.6 all-to-all-start
  30.1 17.2 %all_gather.29 = bf16[2048,128]{1,0:T(8,128)(2,1)S(1)} all-gather(bf16[512,128]{1,0:T(8,128)(2,1)} %param.14), channel_id=1, replica_groups=mesh['rep'=2,'fs'=4,'tp'=4] {'fs'}, dimensions={0}, use_global_device_ids=true | all-gather | bytes 655360 | tf_op jit(solution)/shard_map/all_gather | solution.py:131
  47.3 15.8 %all_gather.30 = bf16[2048,128]{1,0:T(8,128)(2,1)S(1)} all-gather(bf16[512,128]{1,0:T(8,128)(2,1)S(1)} %copy-done.5), channel_id=1, replica_groups=mesh['rep'=2,'fs'=4,'tp'=4] {'fs'}, dimensions={0}, use_global_device_ids=true | all-gather | bytes 655360 | tf_op jit(solution)/shard_map/all_gather | solution.py:132
  63.1 15.8 %all_gather.28 = bf16[2048,128]{1,0:T(8,128)(2,1)S(1)} all-gather(bf16[512,128]{1,0:T(8,128)(2,1)S(1)} %copy-done.6), channel_id=1, replica_groups=mesh['rep'=2,'fs'=4,'tp'=4] {'fs'}, dimensions={0}, use_global_device_ids=true | all-gather | bytes 655360 | tf_op jit(solution)/shard_map/all_gather | solution.py:133
  78.9 0.7 multiply_exponential_fusion
  79.6 0.8 fusion.34
  80.4 15.4 %all_gather.31 = bf16[2048,128]{1,0:T(8,128)(2,1)} all-gather(bf16[512,128]{1,0:T(8,128)(2,1)S(1)} %copy-done.7), channel_id=1, replica_groups=mesh['rep'=2,'fs'=4,'tp'=4] {'fs'}, dimensions={0}, use_global_device_ids=true | all-gather | bytes 655360 | tf_op jit(solution)/shard_map/all_gather | solution.py:134
  95.8 0.7 exponential_select_fusion
  96.5 1.0 copy.71
  97.5 1.8 fusion.14
  99.3 1.8 fusion.16
  101.2 0.6 fusion.40
  101.9 0.6 fusion.41
  102.5 0.8 subtract_convert_fusion
  104.3 1.1 reshape.278
  105.3 1.0 copy.59
  106.3 0.6 convolution_convert_fusion.1
  107.0 0.6 copy-done.4
  107.8 1.9 multiply_bitcast_fusion.1
  109.7 3.4 while.13
  110.2 0.7 constant_dynamic-update-slice_fusion.6
  110.9 0.5 convolution_add_fusion.3
  111.9 0.7 constant_dynamic-update-slice_fusion.6
  112.6 0.5 convolution_add_fusion.3
  113.1 1.8 fusion.39
  116.0 1.6 multiply_convert_fusion.1
  117.6 7.5 %all_gather.32 = bf16[384,512]{1,0:T(8,128)(2,1)S(1)} all-gather(bf16[384,128]{1,0:T(8,128)(2,1)S(1)} %multiply_convert_fusion.1), channel_id=1, replica_groups=mesh['rep'=2,'fs'=4,'tp'=4] {'tp'}, dimensions={1}, use_global_device_ids=true | all-gather | bytes 491520 | tf_op jit(solution)/shard_map/all_gather | solution.py:145
  125.1 2.1 fusion.23
  127.3 0.7 all-gather.8.cloned.1.call-update
  128.0 1.1 collective-permute-start
  129.1 2.8 collective-permute-start.1
  131.9 62.1 %collective-permute-done = bf16[512,2048]{1,0:T(8,128)(2,1)} collective-permute-done((bf16[512,2048]{1,0:T(8,128)(2,1)S(1)}, bf16[512,2048]{1,0:T(8,128)(2,1)}, u32[]{:S(2)}, u32[]{:S(2)}) %collective-permute-start) | collective-permute-done | bytes 2097184 | tf_op jit(solution)/shard_map/ppermute | solution.py:19
  194.0 25.4 %collective-permute-start.2 = (bf16[512,2048]{1,0:T(8,128)(2,1)}, bf16[512,2048]{1,0:T(8,128)(2,1)}, u32[]{:S(2)}, u32[]{:S(2)}) collective-permute-start(bf16[512,2048]{1,0:T(8,128)(2,1)} %collective-permute-done), channel_id=1, source_target_pairs={{0,4},{4,8},{8,12},{12,0},{1,5},{5,9},{9,13},{13,1},{2,6},{6,10},{... | collective-permute-start | bytes 6291464 | tf_op jit(solution)/shard_map/ppermute | solution.py:19
  219.5 4.3 broadcast_in_dim.25
  223.7 1.5 constant_dynamic-update-slice_fusion.4
  225.3 3.1 constant_dynamic-update-slice_fusion.3
  228.4 108.9 %collective-permute-done.1 = bf16[512,2048]{1,0:T(8,128)(2,1)} collective-permute-done((bf16[512,2048]{1,0:T(8,128)(2,1)S(1)}, bf16[512,2048]{1,0:T(8,128)(2,1)}, u32[]{:S(2)}, u32[]{:S(2)}) %collective-permute-start.1) | collective-permute-done | bytes 2097184 | tf_op jit(solution)/shard_map/ppermute | solution.py:22
  337.3 3.2 constant_dynamic-update-slice_fusion.2
  340.5 32.7 %collective-permute-done.2 = bf16[512,2048]{1,0:T(8,128)(2,1)} collective-permute-done((bf16[512,2048]{1,0:T(8,128)(2,1)}, bf16[512,2048]{1,0:T(8,128)(2,1)}, u32[]{:S(2)}, u32[]{:S(2)}) %collective-permute-start.2) | collective-permute-done | bytes 2097184 | tf_op jit(solution)/shard_map/ppermute | solution.py:19
  373.2 3.2 constant_dynamic-update-slice_fusion.1
  376.3 1.8 fusion.17
  378.1 24.5 %all-gather.8.cloned.1.call-done = bf16[2048,2048]{1,0:T(8,128)(2,1)} async-done(((bf16[2048,512]{1,0:T(8,128)(2,1)}), bf16[2048,2048]{1,0:T(8,128)(2,1)}) %all-gather.8.cloned.1.call-update) | async-done | bytes 8388624 | tf_op jit(solution)/shard_map/all_gather | solution.py:157
  402.6 14.1 %convolution_convert_fusion = bf16[384,2048]{1,0:T(8,128)(2,1)} fusion(bf16[2048,2048]{1,0:T(8,128)(2,1)} %all-gather.8.cloned.1.call-done, bf16[2048,2048]{1,0:T(8,128)(2,1)} %constant_dynamic-update-slice_fusion.1, bf16[384,2048]{1,0:T(8,128)(2,1)} %all-gather.6.cloned.1.call-done, f32[2048]{0:T(1024)S(1)} %copy-done.12, f32[384]{0:T(512)S(1)} %add_rsqrt_fusion.1), kind=kOutput, calls=%fused_computation.28 | convolution fusion | flops 6448742400 | bytes 19932672 | tf_op jit(solution)/shard_map/dot_general | solution.py:155
  416.8 26.8 %reduce-scatter.2.cloned.1.call-done = bf16[384,512]{1,0:T(8,128)(2,1)} async-done(((bf16[384,2048]{1,0:T(8,128)(2,1)}), bf16[384,512]{1,0:T(8,128)(2,1)}) %reduce-scatter.2.cloned.1.call-update) | async-done | bytes 393232 | tf_op jit(solution)/shard_map/reduce_scatter | solution.py:160
  443.6 1.8 add_convert_fusion
  (73 shorter events, 3.5 us)
Async XLA Ops:
  6.5 40.7 %copy-start.5 = (bf16[512,128]{1,0:T(8,128)(2,1)S(1)}, bf16[512,128]{1,0:T(8,128)(2,1)}, u32[]{:S(2)}) copy-start(bf16[512,128]{1,0:T(8,128)(2,1)} %param.15) | copy-start | bytes 393220
  6.5 56.6 %copy-start.6 = (bf16[512,128]{1,0:T(8,128)(2,1)S(1)}, bf16[512,128]{1,0:T(8,128)(2,1)}, u32[]{:S(2)}) copy-start(bf16[512,128]{1,0:T(8,128)(2,1)} %param.16) | copy-start | bytes 393220
  6.5 73.8 %copy-start.7 = (bf16[512,128]{1,0:T(8,128)(2,1)S(1)}, bf16[512,128]{1,0:T(8,128)(2,1)}, u32[]{:S(2)}) copy-start(bf16[512,128]{1,0:T(8,128)(2,1)} %param.17) | copy-start | bytes 393220
  6.5 91.0 %all-gather.4.cloned.1.call-start = ((), (), s32[]{:S(2)}) async-start(), calls=%async_computation.2 | async-start | bytes 1966080 | tf_op jit(solution)/shard_map/all_gather | solution.py:127
  26.3 73.0 %copy-start.9 = (f32[2048]{0:T(1024)S(1)}, f32[2048]{0:T(1024)}, u32[]{:S(2)}) copy-start(f32[2048]{0:T(1024)} %param.13) | copy-start | bytes 24580
  26.3 70.2 %all-to-all-start = ((bf16[128,4,512]{0,2,1:T(8,128)(2,1)}), bf16[128,4,512]{0,2,1:T(8,128)(2,1)S(1)}, u32[]{:S(2)}, u32[]{:S(2)}) async-start(bf16[128,4,512]{0,2,1:T(8,128)(2,1)} %bitcast.7), calls=%async_computation | async-start | bytes 1048576 | tf_op jit(solution)/shard_map/all_to_all | solution.py:143
  29.9 346.4 %all-gather.6.cloned.1.call-start = ((), (), s32[]{:S(2)}) async-start(), calls=%async_computation.3 | async-start | bytes 1966080 | tf_op jit(solution)/shard_map/all_gather | solution.py:150
  101.8 0.8 copy-start.8
  103.3 4.3 copy-start.11
  103.6 4.2 copy-start.10
  103.9 3.9 copy-start.3
  107.0 0.7 copy-start.4
  114.9 10.2 %copy-start.2 = (bf16[4,128,512]{2,1,0:T(8,128)(2,1)S(1)}, bf16[4,128,512]{2,1,0:T(8,128)(2,1)}, u32[]{:S(2)}) copy-start(bf16[4,128,512]{2,1,0:T(8,128)(2,1)} %copy.71) | copy-start | bytes 1572868
  117.6 10.4 %copy-start.1 = (bf16[512,2048]{1,0:T(8,128)(2,1)S(1)}, bf16[512,2048]{1,0:T(8,128)(2,1)}, u32[]{:S(2)}) copy-start(bf16[512,2048]{1,0:T(8,128)(2,1)} %param.20) | copy-start | bytes 6291460
  127.2 275.4 %all-gather.8.cloned.1.call-start = ((), (), s32[]{:S(2)}) async-start(), calls=%async_computation.4 | async-start | bytes 10485760 | tf_op jit(solution)/shard_map/all_gather | solution.py:157
  128.0 315.6 %reduce-scatter.2.cloned.1.call-start = ((), (), s32[]{:S(2)}) async-start(), calls=%async_computation.5 | async-start | bytes 1966080 | tf_op jit(solution)/shard_map/reduce_scatter | solution.py:160
  128.0 66.0 %collective-permute-start = (bf16[512,2048]{1,0:T(8,128)(2,1)S(1)}, bf16[512,2048]{1,0:T(8,128)(2,1)}, u32[]{:S(2)}, u32[]{:S(2)}) collective-permute-start(bf16[512,2048]{1,0:T(8,128)(2,1)S(1)} %copy-done.1), channel_id=1, source_target_pairs={{0,4},{4,8},{8,12},{12,0},{1,5},{5,9},{9,13},{13,1},{2,6},{6,10},{... | collective-permute-start | bytes 6291464 | tf_op jit(solution)/shard_map/ppermute | solution.py:19
  129.1 208.2 %collective-permute-start.1 = (bf16[512,2048]{1,0:T(8,128)(2,1)S(1)}, bf16[512,2048]{1,0:T(8,128)(2,1)}, u32[]{:S(2)}, u32[]{:S(2)}) collective-permute-start(bf16[512,2048]{1,0:T(8,128)(2,1)S(1)} %copy-done.1), channel_id=1, source_target_pairs={{0,12},{4,0},{8,4},{12,8},{1,13},{5,1},{9,5},{13,9},{2,14},{6,2},{... | collective-permute-start | bytes 6291464 | tf_op jit(solution)/shard_map/ppermute | solution.py:22
  194.0 179.1 %collective-permute-start.2 = (bf16[512,2048]{1,0:T(8,128)(2,1)}, bf16[512,2048]{1,0:T(8,128)(2,1)}, u32[]{:S(2)}, u32[]{:S(2)}) collective-permute-start(bf16[512,2048]{1,0:T(8,128)(2,1)} %collective-permute-done), channel_id=1, source_target_pairs={{0,4},{4,8},{8,12},{12,0},{1,5},{5,9},{9,13},{13,1},{2,6},{6,10},{... | collective-permute-start | bytes 6291464 | tf_op jit(solution)/shard_map/ppermute | solution.py:19
  340.5 62.2 %copy-start.12 = (f32[2048]{0:T(1024)S(1)}, f32[2048]{0:T(1024)}, u32[]{:S(2)}) copy-start(f32[2048]{0:T(1024)} %param.19) | copy-start | bytes 24580
  378.1 65.5 %copy-start = (bf16[384,512]{1,0:T(8,128)(2,1)S(1)}, bf16[384,512]{1,0:T(8,128)(2,1)}, u32[]{:S(2)}) copy-start(bf16[384,512]{1,0:T(8,128)(2,1)} %fusion.23) | copy-start | bytes 1179652
Sparse Core Ops, SparseCore 0:
  8.9 22.3 all-gather.3
  127.3 19.9 all-gather.5
  148.9 253.7 all-gather.7
  416.9 26.6 reduce-scatter.1
